TPU v7x, 256 devices: a whole 4x4x8 slice. The times are simulated.
256 devices in a mesh: sp: 64 (over z, x, core), tp: 4 (over y).
Axes of the slice: x: 4, y: 4, z: 8, core: 2. Of those that a mesh axis runs over, the one named last changes fastest.
Arguments:
- stream: bfloat16 [32768, 2048], P(('sp', 'tp')), may hold values from -6 to 6
- pool_in: bfloat16 [32768, 1024], P('sp', 'tp'), may hold values from -6 to 6
- doc_ids: int32 [32768], P('sp'), may hold values from 0 to 7, never falling along the last dimension, each value on 1 to 8192 neighbouring positions
- pool_map: bfloat16 [4, 256, 512], P('tp'), may hold values from -0.375 to 0.375
- pool_scale: float32 [2048], P('tp'), may hold values from 0.1 to 1.9
- out_weight: bfloat16 [2048, 2048], P('tp'), may hold values from -0.125 to 0.125
- norm_gain: float32 [2048], replicated, may hold values from 0.1 to 1.9
- routes: int32 [32768, 2], P('sp'), may hold values from 0 to 63, all different within a row; in each aligned block of 128 rows (0 to 127, 128 to 255, ...) at most 6 rows name the same one
- route_weight: float32 [32768, 2], P(('sp', 'tp')), may hold values from 0.2 to 1
- expert_gate: bfloat16 [64, 2048, 1024], P('sp', None, 'tp'), may hold values from -0.125 to 0.125
- expert_up: bfloat16 [64, 2048, 1024], P('sp', None, 'tp'), may hold values from -0.125 to 0.125
- expert_down: bfloat16 [64, 1024, 2048], P('sp', 'tp'), may hold values from -0.1875 to 0.1875
Outputs:
- result: bfloat16 [32768, 2048], P(('sp', 'tp'))
Inputs may be any that keep to these rules, and one draw needn't show every extreme that they name: `routes`: each token names 2 different experts; in each aligned block of 128 rows no expert is named by more than 6 rows, a bound that some block reaches. `doc_ids`: never falling; each document holds at most 8192 positions.
All inputs are finite; a program needn't handle non-finite values.
Results may differ from a plain program's by a relative error of at most 0.014.
Values may be sent and summed in bfloat16 or wider, within the bound.
A program may use at most 64 MiB of HBM per device.

v0:
```python
import jax
import jax.numpy as jnp
from jax import lax
from jax.sharding import PartitionSpec as P

SPAN = 16
EPS = 1e-06


def passed_along(value, axis, by):
    length = lax.axis_size(axis)
    pairs = [(i, i + by) for i in range(length) if 0 <= i + by < length]
    return lax.ppermute(value, axis, pairs)


def cut_along(value, dim, length):
    before, after = (value.shape[:dim], value.shape[dim + 1 :])
    return jnp.moveaxis(value.reshape(*before, length, -1, *after), dim, 0)


def sum_at_owner(value, axis, dim):
    length = lax.axis_size(axis)
    tiles = lax.all_to_all(cut_along(value, dim, length), axis, 0, 0, tiled=True)
    return jnp.sum(tiles.astype(jnp.float32), axis=0)


def slot_table(route_block, expert_count, capacity, top_count):
    flattened = route_block.reshape(-1)
    one_hot = (flattened[:, None] == jnp.arange(expert_count, dtype=jnp.int32)[None, :]).astype(
        jnp.int32
    )
    ranking = jnp.sum((jnp.cumsum(one_hot, axis=0) - one_hot) * one_hot, axis=1)
    target_slot = flattened * capacity + ranking
    matches = target_slot[None, :] == jnp.arange(expert_count * capacity, dtype=jnp.int32)[:, None]
    sources = jnp.sum(
        jnp.where(matches, jnp.arange(flattened.shape[0], dtype=jnp.int32)[None, :], 0), axis=1
    )
    filled = jnp.any(matches, axis=1)
    return (target_slot, sources // top_count, filled)


def per_device(
    stream,
    pool_in,
    doc_ids,
    pool_map,
    pool_scale,
    out_weight,
    norm_gain,
    routes,
    route_weight,
    expert_gate,
    expert_up,
    expert_down,
):
    row_count = pool_in.shape[0]
    model_width = stream.shape[1]
    top_count = routes.shape[1]
    tp_count = lax.axis_size("tp")
    expert_count = lax.axis_size("sp")
    quarter = row_count // tp_count
    capacity = max(2, 3 * top_count * quarter // (2 * expert_count))
    all_gate = lax.all_gather(expert_gate, "tp", axis=0, tiled=True)
    all_up = lax.all_gather(expert_up, "tp", axis=0, tiled=True)
    all_down = lax.all_gather(expert_down, "tp", axis=0, tiled=True)
    reach_rows = SPAN - 1
    tail_rows = (
        pool_in[row_count - reach_rows :],
        doc_ids[row_count - reach_rows :].astype(jnp.bfloat16),
    )
    prior_rows, prior_docs = passed_along((tail_rows[0], tail_rows[1]), "sp", 1)
    extended = jnp.concatenate([prior_rows, pool_in], axis=0).astype(jnp.float32)
    extended_docs = jnp.concatenate([prior_docs.astype(jnp.float32), doc_ids.astype(jnp.float32)])
    own_docs = doc_ids.astype(jnp.float32)
    window = jnp.left_shift(jnp.int32(2), lax.axis_index("tp"))
    positions = lax.axis_index("sp") * row_count + jnp.arange(row_count, dtype=jnp.int32)
    running = jnp.zeros(pool_in.shape, jnp.float32)
    counts = jnp.zeros((row_count,), jnp.float32)
    for offset in range(reach_rows + 1):
        begin_row = reach_rows - offset
        piece_rows = extended[begin_row : begin_row + row_count]
        piece_docs = extended_docs[begin_row : begin_row + row_count]
        in_window = (offset < window) & (positions - offset >= 0) & (piece_docs == own_docs)
        running = running + jnp.where(in_window[:, None], piece_rows, 0.0)
        counts = counts + in_window.astype(jnp.float32)
    pooled = (running / counts[:, None] - pool_in.astype(jnp.float32)).astype(jnp.bfloat16)
    branch = (jnp.dot(pooled, pool_map[0], preferred_element_type=jnp.float32) * pool_scale).astype(
        jnp.bfloat16
    )
    projected = sum_at_owner(
        jnp.dot(branch, out_weight, preferred_element_type=jnp.float32).astype(jnp.bfloat16),
        "tp",
        0,
    )
    mixed_rows = (stream.astype(jnp.float32) + projected).astype(jnp.bfloat16)
    mixed_up = mixed_rows.astype(jnp.float32)
    normed = (
        mixed_up * lax.rsqrt(jnp.mean(mixed_up * mixed_up, axis=1, keepdims=True) + EPS) * norm_gain
    ).astype(jnp.bfloat16)
    own_routes = lax.dynamic_slice_in_dim(routes, lax.axis_index("tp") * quarter, quarter, 0)
    own_slots, own_sources, own_filled = slot_table(own_routes, expert_count, capacity, top_count)
    token_index = own_sources.reshape(expert_count, 1, capacity)
    filled_slots = own_filled.reshape(expert_count, 1, capacity)
    dispatch = jnp.where(filled_slots[..., None], normed[token_index], jnp.zeros((), jnp.bfloat16))
    arrived = lax.all_to_all(dispatch, "sp", split_axis=0, concat_axis=0, tiled=True)
    stacked = arrived.reshape(-1, model_width)
    expert_sum = jnp.zeros(stacked.shape, jnp.float32)
    for part in range(tp_count):
        gate_pre = jnp.dot(stacked, all_gate[part], preferred_element_type=jnp.float32)
        up_pre = jnp.dot(stacked, all_up[part], preferred_element_type=jnp.float32)
        hidden = (jax.nn.silu(gate_pre) * up_pre).astype(jnp.bfloat16)
        part_out = jnp.dot(hidden, all_down[part], preferred_element_type=jnp.float32)
        expert_sum = expert_sum + part_out.astype(jnp.bfloat16).astype(jnp.float32)
    summed = expert_sum.astype(jnp.bfloat16).reshape(arrived.shape)
    returned = lax.all_to_all(summed, "sp", split_axis=0, concat_axis=0, tiled=True)
    outputs = returned.reshape(expert_count * capacity, model_width)
    picked = outputs[own_slots].astype(jnp.float32).reshape(quarter, top_count, model_width)
    combined = jnp.sum(route_weight[:, :, None] * picked, axis=1)
    return (mixed_up + combined).astype(jnp.bfloat16)


def solution(mesh):
    in_specs = (
        P(("sp", "tp"), None),
        P("sp", "tp"),
        P("sp"),
        P("tp", None, None),
        P("tp"),
        P("tp", None),
        P(),
        P("sp", None),
        P(("sp", "tp"), None),
        P("sp", None, "tp"),
        P("sp", None, "tp"),
        P("sp", "tp", None),
    )
    out_specs = P(("sp", "tp"), None)
    return jax.shard_map(
        per_device, mesh=mesh, in_specs=in_specs, out_specs=out_specs, check_vma=False
    )
```

profile of v0, /device:TPU:2, one launch (start us, length us, event | category | flops | bytes accessed | tf_op | source)
XLA Modules:
  0.0 302.6 jit_solution(7720405257235284247)
XLA Ops:
  8.1 1.9 collective-permute-start.1
  10.1 3.5 %collective-permute-start = (bf16[15,256]{1,0:T(8,128)(2,1)S(1)}, bf16[15,256]{1,0:T(8,128)(2,1)S(1)}, u32[]{:S(2)}, u32[]{:S(2)}) collective-permute-start(bf16[15,256]{1,0:T(8,128)(2,1)S(1)} %slice.142), channel_id=1, source_target_pairs={{0,4},{4,8},{8,12},{12,16},{16,20},{20,24},{24,28},{28,32},{32,36}... | collective-permute-start | bytes 23048 | tf_op jit(solution)/shard_map/ppermute | solution.py:13
  15.1 4.4 %convolution_convert_fusion = bf16[512,2048]{1,0:T(8,128)(2,1)} fusion(bf16[512,2048]{1,0:T(8,128)(2,1)S(1)} %copy-done, f32[512]{0:T(512)S(1)} %copy-done.8, bf16[512,256]{1,0:T(8,128)(2,1)S(1)} %copy-done.2, f32[527,256]{1,0:T(8,128)S(1)} %maximum_convert_fusion, bf16[1,256,512]{2,1,0:T(8,128)(2,1)S(1)} %copy-done.7, f32[512]{0:T(512)S(1)} %get-tuple-element.9, ...), kind=kOutput, calls=%fused_computation.4 | convolution fusion | flops 1214119936 | bytes 13119488 | tf_op jit(solution)/shard_map/dot_general | solution.py:91
  19.6 4.5 %all-to-all-start = ((bf16[4,128,2048]{2,1,0:T(8,128)(2,1)}), bf16[4,128,2048]{2,1,0:T(8,128)(2,1)}, u32[]{:S(2)}, u32[]{:S(2)}) async-start(bf16[4,128,2048]{2,1,0:T(8,128)(2,1)} %bitcast.84), calls=%async_computation | async-start | bytes 4194304 | tf_op jit(solution)/shard_map/all_to_all | solution.py:23
  27.7 45.3 %all-to-all-done = bf16[4,128,2048]{2,1,0:T(8,128)(2,1)} async-done(((bf16[4,128,2048]{2,1,0:T(8,128)(2,1)}), bf16[4,128,2048]{2,1,0:T(8,128)(2,1)}, u32[]{:S(2)}, u32[]{:S(2)}) %all-to-all-start) | async-done | bytes 2097184 | tf_op jit(solution)/shard_map/all_to_all | solution.py:23
  73.0 2.1 convert_reduce_fusion
  76.6 3.1 %gather_fusion = bf16[384,2048]{1,0:T(8,128)(2,1)} fusion(bf16[128,2048]{1,0:T(8,128)(2,1)S(1)} %fusion.7, s32[1024]{0:T(1024)S(1)} %pad_clamp_fusion.1), kind=kCustom, calls=%fused_computation | custom fusion | bytes 3147264 | tf_op jit(solution)/shard_map/gather | solution.py:104
  79.8 3.7 %reshape.213 = bf16[64,1,6,2048]{3,2,0,1:T(8,128)(2,1)} reshape(bf16[384,2048]{1,0:T(8,128)(2,1)} %gather_fusion) | data formatting | bytes 3145728 | tf_op jit(solution)/shard_map/gather | solution.py:104
  85.3 63.9 %all_to_all.15 = bf16[64,1,6,2048]{3,2,1,0:T(8,128)(2,1)} all-to-all(bf16[64,1,6,2048]{3,2,1,0:T(8,128)(2,1)S(1)} %select_bitcast_fusion), channel_id=1, replica_groups=mesh['sp'=64,'tp'=4] {'sp'}, dimensions={0} | all-to-all | bytes 3145728 | tf_op jit(solution)/shard_map/all_to_all | solution.py:105
  149.2 3.7 %reshape.208 = bf16[384,2048]{1,0:T(8,128)(2,1)} reshape(bf16[64,1,6,2048]{3,2,1,0:T(8,128)(2,1)} %all_to_all.15) | data formatting | bytes 3145728 | tf_op jit(solution)/shard_map/reshape | solution.py:106
  152.9 3.3 %fusion.9 = f32[384,256]{1,0:T(8,128)} fusion(bf16[384,2048]{1,0:T(8,128)(2,1)} %reshape.208, bf16[4,2048,256]{2,1,0:T(8,128)(2,1)} %all-gather.4.cloned.1.call-done), kind=kOutput, calls=%fused_computation.31 | convolution fusion | flops 402653184 | bytes 3014656 | tf_op jit(solution)/shard_map/dot_general | solution.py:109
  156.2 2.7 fusion.10
  160.9 29.9 %all-gather.8.cloned.1.call-done = bf16[4,256,2048]{2,1,0:T(8,128)(2,1)} async-done(((bf16[1,256,2048]{2,1,0:T(8,128)(2,1)}), bf16[4,256,2048]{2,1,0:T(8,128)(2,1)}) %all-gather.8.cloned.1.call-update) | async-done | bytes 4194320 | tf_op jit(solution)/shard_map/all_gather | solution.py:65
  190.8 5.2 %convolution_convert_fusion.3 = bf16[384,2048]{1,0:T(8,128)(2,1)} fusion(bf16[384,2048]{1,0:T(8,128)(2,1)} %reshape.208, bf16[4,256,2048]{2,1,0:T(8,128)(2,1)} %all-gather.8.cloned.1.call-done, bf16[4,2048,256]{2,1,0:T(8,128)(2,1)} %all-gather.6.cloned.1.call-done, f32[384,256]{1,0:T(8,128)} %fusion.11), kind=kOutput, calls=%fused_computation.7 | convolution fusion | flops 806682624 | bytes 5636096 | tf_op jit(solution)/shard_map/dot_general | solution.py:112
  196.0 5.1 %convolution_convert_fusion.2 = bf16[384,2048]{1,0:T(8,128)(2,1)} fusion(bf16[384,2048]{1,0:T(8,128)(2,1)} %reshape.208, bf16[4,256,2048]{2,1,0:T(8,128)(2,1)} %all-gather.8.cloned.1.call-done, bf16[4,2048,256]{2,1,0:T(8,128)(2,1)} %all-gather.6.cloned.1.call-done, f32[384,256]{1,0:T(8,128)} %fusion.10), kind=kOutput, calls=%fused_computation.6 | convolution fusion | flops 806682624 | bytes 5636096 | tf_op jit(solution)/shard_map/dot_general | solution.py:112
  201.1 5.1 %convolution_convert_fusion.1 = bf16[384,2048]{1,0:T(8,128)(2,1)} fusion(bf16[384,2048]{1,0:T(8,128)(2,1)} %reshape.208, bf16[4,256,2048]{2,1,0:T(8,128)(2,1)} %all-gather.8.cloned.1.call-done, bf16[4,2048,256]{2,1,0:T(8,128)(2,1)} %all-gather.6.cloned.1.call-done, f32[384,256]{1,0:T(8,128)} %fusion.9), kind=kOutput, calls=%fused_computation.5 | convolution fusion | flops 806682624 | bytes 5636096 | tf_op jit(solution)/shard_map/dot_general | solution.py:112
  206.2 6.4 %add_convert_fusion = bf16[384,2048]{1,0:T(8,128)(2,1)} fusion(bf16[384,2048]{1,0:T(8,128)(2,1)} %convolution_convert_fusion.1, bf16[384,2048]{1,0:T(8,128)(2,1)} %convolution_convert_fusion.2, bf16[384,2048]{1,0:T(8,128)(2,1)} %convolution_convert_fusion.3, bf16[4,256,2048]{2,1,0:T(8,128)(2,1)} %all-gather.8.cloned.1.call-done, ...), kind=kOutput, calls=%fused_computation.3 | convolution fusion | flops 812974080 | bytes 10354688 | tf_op jit(solution)/shard_map/dot_general | solution.py:112
  212.6 3.7 %reshape.209 = bf16[64,1,6,2048]{3,2,0,1:T(8,128)(2,1)} reshape(bf16[384,2048]{1,0:T(8,128)(2,1)} %add_convert_fusion) | data formatting | bytes 3145728 | tf_op jit(solution)/shard_map/reshape | solution.py:114
  216.3 10.9 %all-to-all-start.2 = ((bf16[64,1,6,2048]{3,2,1,0:T(8,128)(2,1)}), bf16[64,1,6,2048]{3,2,1,0:T(8,128)(2,1)}, u32[]{:S(2)}, u32[]{:S(2)}) async-start(bf16[64,1,6,2048]{3,2,1,0:T(8,128)(2,1)} %bitcast.83), calls=%async_computation.2 | async-start | bytes 4194304 | tf_op jit(solution)/shard_map/all_to_all | solution.py:115
  227.6 50.7 %all-to-all-done.2 = bf16[64,1,6,2048]{3,2,1,0:T(8,128)(2,1)} async-done(((bf16[64,1,6,2048]{3,2,1,0:T(8,128)(2,1)}), bf16[64,1,6,2048]{3,2,1,0:T(8,128)(2,1)}, u32[]{:S(2)}, u32[]{:S(2)}) %all-to-all-start.2) | async-done | bytes 1572896 | tf_op jit(solution)/shard_map/all_to_all | solution.py:115
  278.3 3.7 %reshape.210 = bf16[384,2048]{1,0:T(8,128)(2,1)} reshape(bf16[64,1,6,2048]{3,2,1,0:T(8,128)(2,1)} %all-to-all-done.2) | data formatting | bytes 3145728 | tf_op jit(solution)/shard_map/reshape | solution.py:116
  282.0 4.9 %gather_fusion.1 = bf16[256,2048]{1,0:T(8,128)(2,1)} fusion(bf16[384,2048]{1,0:T(8,128)(2,1)} %reshape.210, s32[1024]{0:T(1024)S(1)} %pad_clamp_fusion), kind=kCustom, calls=%fused_computation.1 | custom fusion | bytes 2098176 | tf_op jit(solution)/shard_map/gather | solution.py:117
  286.9 3.4 %reshape.211 = f32[128,2,2048]{2,1,0:T(2,128)} reshape(bf16[256,2048]{1,0:T(8,128)(2,1)} %gather_fusion.1) | data formatting | bytes 3145728 | tf_op jit(solution)/shard_map/convert_element_type | solution.py:117
  290.3 4.8 %multiply_reduce_fusion = f32[128,2048]{1,0:T(8,128)S(1)} fusion(f32[128,2,2048]{2,1,0:T(2,128)} %reshape.211, f32[128,2]{1,0:T(8,128)S(1)} %copy.26), kind=kLoop, calls=%fused_computation.9 | loop fusion | flops 786432 | bytes 3146752 | tf_op jit(solution)/shard_map/reduce_sum | solution.py:118
  (65 shorter events, 13.2 us)
Async XLA Ops:
  6.5 8.6 %copy-start = (bf16[512,2048]{1,0:T(8,128)(2,1)S(1)}, bf16[512,2048]{1,0:T(8,128)(2,1)}, u32[]{:S(2)}) copy-start(bf16[512,2048]{1,0:T(8,128)(2,1)} %param.17) | copy-start | bytes 6291460
  6.5 1.5 copy-start.4
  6.5 3.5 %copy-start.2 = (bf16[512,256]{1,0:T(8,128)(2,1)S(1)}, bf16[512,256]{1,0:T(8,128)(2,1)}, u32[]{:S(2)}) copy-start(bf16[512,256]{1,0:T(8,128)(2,1)} %param.13) | copy-start | bytes 786436
  6.5 8.6 %copy-start.8 = (f32[512]{0:T(512)S(1)}, f32[512]{0:T(512)}, u32[]{:S(2)}) copy-start(f32[512]{0:T(512)} %param.16) | copy-start | bytes 6148
  6.5 8.6 %copy-start.7 = (bf16[1,256,512]{2,1,0:T(8,128)(2,1)S(1)}, bf16[1,256,512]{2,1,0:T(8,128)(2,1)}, u32[]{:S(2)}) copy-start(bf16[1,256,512]{2,1,0:T(8,128)(2,1)} %param.15) | copy-start | bytes 786436
  6.5 146.4 %all-gather.4.cloned.1.call-start = ((), (), s32[]{:S(2)}) async-start(), calls=%async_computation.3 | async-start | bytes 5242880 | tf_op jit(solution)/shard_map/all_gather | solution.py:63
  7.3 153.6 %all-gather.6.cloned.1.call-start = ((), (), s32[]{:S(2)}) async-start(), calls=%async_computation.4 | async-start | bytes 5242880 | tf_op jit(solution)/shard_map/all_gather | solution.py:64
  8.1 5.5 %collective-permute-start.1 = (bf16[15]{0:T(256)(128)(2,1)S(1)}, bf16[15]{0:T(256)(128)(2,1)S(1)}, u32[]{:S(2)}, u32[]{:S(2)}) collective-permute-start(bf16[15]{0:T(256)(128)(2,1)S(1)} %slice.144), channel_id=1, source_target_pairs={{0,4},{4,8},{8,12},{12,16},{16,20},{20,24},{24,28},{28,32},{32,36}... | collective-permute-start | bytes 98 | tf_op jit(solution)/shard_map/ppermute | solution.py:13
  10.1 5.0 %collective-permute-start = (bf16[15,256]{1,0:T(8,128)(2,1)S(1)}, bf16[15,256]{1,0:T(8,128)(2,1)S(1)}, u32[]{:S(2)}, u32[]{:S(2)}) collective-permute-start(bf16[15,256]{1,0:T(8,128)(2,1)S(1)} %slice.142), channel_id=1, source_target_pairs={{0,4},{4,8},{8,12},{12,16},{16,20},{20,24},{24,28},{28,32},{32,36}... | collective-permute-start | bytes 23048 | tf_op jit(solution)/shard_map/ppermute | solution.py:13
  19.6 53.4 %all-to-all-start = ((bf16[4,128,2048]{2,1,0:T(8,128)(2,1)}), bf16[4,128,2048]{2,1,0:T(8,128)(2,1)}, u32[]{:S(2)}, u32[]{:S(2)}) async-start(bf16[4,128,2048]{2,1,0:T(8,128)(2,1)} %bitcast.84), calls=%async_computation | async-start | bytes 4194304 | tf_op jit(solution)/shard_map/all_to_all | solution.py:23
  24.0 166.8 %all-gather.8.cloned.1.call-start = ((), (), s32[]{:S(2)}) async-start(), calls=%async_computation.5 | async-start | bytes 5242880 | tf_op jit(solution)/shard_map/all_gather | solution.py:65
  27.7 48.8 %copy-start.3 = (f32[2048]{0:T(1024)S(1)}, f32[2048]{0:T(1024)}, u32[]{:S(2)}) copy-start(f32[2048]{0:T(1024)} %param.18) | copy-start | bytes 24580
  152.9 3.3 %copy-start.1 = (bf16[384,2048]{1,0:T(8,128)(2,1)S(1)}, bf16[384,2048]{1,0:T(8,128)(2,1)}, u32[]{:S(2)}) copy-start(bf16[384,2048]{1,0:T(8,128)(2,1)} %reshape.208) | copy-start | bytes 4718596
  156.2 2.7 copy-start.6
  216.3 11.1 %copy-start.5 = (f32[128,2]{0,1:T(2,128)S(1)}, f32[128,2]{0,1:T(2,128)}, u32[]{:S(2)}) copy-start(f32[128,2]{0,1:T(2,128)} %param.20) | copy-start | bytes 3076
  216.3 62.0 %all-to-all-start.2 = ((bf16[64,1,6,2048]{3,2,1,0:T(8,128)(2,1)}), bf16[64,1,6,2048]{3,2,1,0:T(8,128)(2,1)}, u32[]{:S(2)}, u32[]{:S(2)}) async-start(bf16[64,1,6,2048]{3,2,1,0:T(8,128)(2,1)} %bitcast.83), calls=%async_computation.2 | async-start | bytes 4194304 | tf_op jit(solution)/shard_map/all_to_all | solution.py:115
Sparse Core Ops, SparseCore 0:
  9.2 75.0 all-gather.3
  86.1 51.7 all-gather.5
  139.7 51.1 all-gather.7
where the time goes:
time: 304 us; the launch traced here: 303 us
  waiting for transfers between devices  129 us (42%)
  blocking collectives  63.9 us (21%)
  matrix products  34.2 us (11%)
  local copies, waits for them, and re-layouts  27.7 us (9%)
  starting transfers between devices  20.9 us (7%)
  between operations  13.4 us (4%)
  other arithmetic  13.3 us (4%)
    all_to_all x1, blocking collectives, per_device(): lax.all_to_all(dispatch, 'sp', split_axis=0, concat_axis=0, tiled=True)  63.9 us
    all_to_all x1, waiting for transfers between devices, per_device(): lax.all_to_all(summed, 'sp', split_axis=0, concat_axis=0, tiled=True)  50.7 us
    all_to_all x1, waiting for transfers between devices, sum_at_owner(): lax.all_to_all(cut_along(value, dim, length), axis, 0, 0, tiled=True)  45.3 us
    all_gather x1, waiting for transfers between devices, per_device(): all_down = lax.all_gather(expert_down, 'tp', axis=0, tiled=True)  29.9 us
    dot_general x4, matrix products, per_device(): jnp.dot(hidden, all_down[part], preferred_element_type=jnp.float32)  21.8 us
    all_to_all x1, starting transfers between devices, per_device(): lax.all_to_all(summed, 'sp', split_axis=0, concat_axis=0, tiled=True)  10.9 us
    dot_general x4, matrix products, per_device(): jnp.dot(stacked, all_gate[part], preferred_element_type=jnp.float32)  7.93 us
    gather x2, local copies, waits for them, and re-layouts, per_device(): normed[token_index]  6.78 us
  transfers between devices with their start and end apart: 7, of which 4 were waited for; matrix products, arithmetic and copies ran while one was open for 11% of the time, Pallas kernels for 0%

commit v1 on v0

--- a/solution.py
+++ b/solution.py
@@ -62,7 +62,9 @@
     capacity = max(2, 3 * top_count * quarter // (2 * expert_count))
     all_gate = lax.all_gather(expert_gate, "tp", axis=0, tiled=True)
     all_up = lax.all_gather(expert_up, "tp", axis=0, tiled=True)
-    all_down = lax.all_gather(expert_down, "tp", axis=0, tiled=True)
+    all_down = lax.all_to_all(
+        jnp.concatenate([expert_down] * lax.psum(1, "tp"), axis=0), "tp", 0, 0, tiled=True
+    )
     reach_rows = SPAN - 1
     tail_rows = (
         pool_in[row_count - reach_rows :],

time: 304 us -> 317 us (1.043)
  waiting for transfers between devices: 129 us -> 135 us
  local copies, waits for them, and re-layouts: 27.7 us -> 30.9 us
    all_to_all x0 -> x1, waiting for transfers between devices: none -> 36 us  [per_device(): lax.all_to_all(jnp.concatenate([expert_down] * lax.psum(1, 'tp'), axis=0)...]
    all_gather x1 -> x0, waiting for transfers between devices: 29.9 us -> none  [per_device(): all_down = lax.all_gather(expert_down, 'tp', axis=0, tiled=True)]
    all_to_all x0 -> x1, starting transfers between devices: none -> 5.12 us  [per_device(): lax.all_to_all(jnp.concatenate([expert_down] * lax.psum(1, 'tp'), axis=0)...]
    all_to_all x1, starting transfers between devices: 10.9 us -> 7.16 us  [per_device(): lax.all_to_all(summed, 'sp', split_axis=0, concat_axis=0, tiled=True)]
  transfers between devices with their start and end apart: 7 -> 7, of which waited for: 4 -> 4; matrix products, arithmetic and copies ran while one was open for 11% -> 12% of each run, Pallas kernels for 0% -> 0%
where the time goes in v1:
time: 317 us; the launch traced here: 315 us
  waiting for transfers between devices  135 us (43%)
  blocking collectives  63.2 us (20%)
  matrix products  34.8 us (11%)
  local copies, waits for them, and re-layouts  30.9 us (10%)
  starting transfers between devices  22.3 us (7%)
  other arithmetic  15.6 us (5%)
  between operations  13.7 us (4%)
    all_to_all x1, blocking collectives, per_device(): lax.all_to_all(dispatch, 'sp', split_axis=0, concat_axis=0, tiled=True)  63.2 us
    all_to_all x1, waiting for transfers between devices, per_device(): lax.all_to_all(summed, 'sp', split_axis=0, concat_axis=0, tiled=True)  50.7 us
    all_to_all x1, waiting for transfers between devices, sum_at_owner(): lax.all_to_all(cut_along(value, dim, length), axis, 0, 0, tiled=True)  46.2 us
    all_to_all x1, waiting for transfers between devices, per_device(): lax.all_to_all(jnp.concatenate([expert_down] * lax.psum(1, 'tp'), axis=0)...  36 us
    dot_general x4, matrix products, per_device(): jnp.dot(hidden, all_down[part], preferred_element_type=jnp.float32)  21.8 us
    dot_general x4, matrix products, per_device(): jnp.dot(stacked, all_gate[part], preferred_element_type=jnp.float32)  7.72 us
    all_to_all x1, starting transfers between devices, per_device(): lax.all_to_all(summed, 'sp', split_axis=0, concat_axis=0, tiled=True)  7.16 us
    gather x2, local copies, waits for them, and re-layouts, per_device(): normed[token_index]  6.83 us
  transfers between devices with their start and end apart: 7, of which 4 were waited for; matrix products, arithmetic and copies ran while one was open for 12% of the time, Pallas kernels for 0%

profile of v1, /device:TPU:2, one launch (start us, length us, event | category | flops | bytes accessed | tf_op | source)
XLA Modules:
  0.0 315.4 jit_solution(10292409412370250174)
XLA Ops:
  10.7 3.5 %collective-permute-start = (bf16[15,256]{1,0:T(8,128)(2,1)S(1)}, bf16[15,256]{1,0:T(8,128)(2,1)S(1)}, u32[]{:S(2)}, u32[]{:S(2)}) collective-permute-start(bf16[15,256]{1,0:T(8,128)(2,1)S(1)} %slice.142), channel_id=1, source_target_pairs={{0,4},{4,8},{8,12},{12,16},{16,20},{20,24},{24,28},{28,32},{32,36}... | collective-permute-start | bytes 23048 | tf_op jit(solution)/shard_map/ppermute | solution.py:13
  16.7 5.3 %convolution_convert_fusion = bf16[512,2048]{1,0:T(8,128)(2,1)} fusion(bf16[512,2048]{1,0:T(8,128)(2,1)S(1)} %copy-done, f32[512]{0:T(512)} %param.16, bf16[512,256]{1,0:T(8,128)(2,1)} %param.13, f32[527,256]{1,0:T(8,128)S(1)} %maximum_convert_fusion, bf16[1,256,512]{2,1,0:T(8,128)(2,1)} %param.15, f32[512]{0:T(512)S(1)} %get-tuple-element.9, ...), kind=kOutput, calls=%fused_computation.4 | convolution fusion | flops 1214119936 | bytes 13119488 | tf_op jit(solution)/shard_map/dot_general | solution.py:93
  22.0 4.5 %all-to-all-start = ((bf16[4,128,2048]{2,1,0:T(8,128)(2,1)}), bf16[4,128,2048]{2,1,0:T(8,128)(2,1)}, u32[]{:S(2)}, u32[]{:S(2)}) async-start(bf16[4,128,2048]{2,1,0:T(8,128)(2,1)} %bitcast.85), calls=%async_computation | async-start | bytes 4194304 | tf_op jit(solution)/shard_map/all_to_all | solution.py:23
  30.2 46.2 %all-to-all-done = bf16[4,128,2048]{2,1,0:T(8,128)(2,1)} async-done(((bf16[4,128,2048]{2,1,0:T(8,128)(2,1)}), bf16[4,128,2048]{2,1,0:T(8,128)(2,1)}, u32[]{:S(2)}, u32[]{:S(2)}) %all-to-all-start) | async-done | bytes 2097184 | tf_op jit(solution)/shard_map/all_to_all | solution.py:23
  80.0 3.1 gather_fusion
  83.2 3.7 %reshape.214 = bf16[64,1,6,2048]{3,2,0,1:T(8,128)(2,1)} reshape(bf16[384,2048]{1,0:T(8,128)(2,1)} %gather_fusion) | data formatting | bytes 3145728 | tf_op jit(solution)/shard_map/gather | solution.py:106
  88.7 63.2 %all_to_all.20 = bf16[64,1,6,2048]{3,2,1,0:T(8,128)(2,1)} all-to-all(bf16[64,1,6,2048]{3,2,1,0:T(8,128)(2,1)S(1)} %select_bitcast_fusion), channel_id=1, replica_groups=mesh['sp'=64,'tp'=4] {'sp'}, dimensions={0} | all-to-all | bytes 3145728 | tf_op jit(solution)/shard_map/all_to_all | solution.py:107
  152.0 2.5 concatenate.11
  154.5 5.1 %all-to-all-start.2 = ((bf16[4,256,2048]{2,1,0:T(8,128)(2,1)}), bf16[4,256,2048]{2,1,0:T(8,128)(2,1)}, u32[]{:S(2)}, u32[]{:S(2)}) async-start(bf16[4,256,2048]{2,1,0:T(8,128)(2,1)} %concatenate.11), calls=%async_computation.2 | async-start | bytes 8388608 | tf_op jit(solution)/shard_map/all_to_all | solution.py:65
  159.6 3.7 %reshape.209 = bf16[384,2048]{1,0:T(8,128)(2,1)} reshape(bf16[64,1,6,2048]{3,2,1,0:T(8,128)(2,1)} %all_to_all.20) | data formatting | bytes 3145728 | tf_op jit(solution)/shard_map/reshape | solution.py:108
  163.3 3.1 fusion.9
  166.4 2.7 fusion.10
  171.0 36.0 %all-to-all-done.2 = bf16[4,256,2048]{2,1,0:T(8,128)(2,1)} async-done(((bf16[4,256,2048]{2,1,0:T(8,128)(2,1)}), bf16[4,256,2048]{2,1,0:T(8,128)(2,1)}, u32[]{:S(2)}, u32[]{:S(2)}) %all-to-all-start.2) | async-done | bytes 4194336 | tf_op jit(solution)/shard_map/all_to_all | solution.py:65
  207.0 5.1 %convolution_convert_fusion.1 = bf16[384,2048]{1,0:T(8,128)(2,1)} fusion(bf16[384,2048]{1,0:T(8,128)(2,1)} %reshape.209, bf16[4,256,2048]{2,1,0:T(8,128)(2,1)} %all-to-all-done.2, bf16[4,2048,256]{2,1,0:T(8,128)(2,1)} %all-gather.5.cloned.1.call-done, f32[384,256]{1,0:T(8,128)} %fusion.9), kind=kOutput, calls=%fused_computation.5 | convolution fusion | flops 806682624 | bytes 5636096 | tf_op jit(solution)/shard_map/dot_general | solution.py:114
  212.2 5.1 %convolution_convert_fusion.2 = bf16[384,2048]{1,0:T(8,128)(2,1)} fusion(bf16[384,2048]{1,0:T(8,128)(2,1)} %reshape.209, bf16[4,256,2048]{2,1,0:T(8,128)(2,1)} %all-to-all-done.2, bf16[4,2048,256]{2,1,0:T(8,128)(2,1)} %all-gather.5.cloned.1.call-done, f32[384,256]{1,0:T(8,128)} %fusion.10), kind=kOutput, calls=%fused_computation.6 | convolution fusion | flops 806682624 | bytes 5636096 | tf_op jit(solution)/shard_map/dot_general | solution.py:114
  217.3 5.1 %convolution_convert_fusion.3 = bf16[384,2048]{1,0:T(8,128)(2,1)} fusion(bf16[384,2048]{1,0:T(8,128)(2,1)} %reshape.209, bf16[4,256,2048]{2,1,0:T(8,128)(2,1)} %all-to-all-done.2, bf16[4,2048,256]{2,1,0:T(8,128)(2,1)} %all-gather.5.cloned.1.call-done, f32[384,256]{1,0:T(8,128)} %fusion.11), kind=kOutput, calls=%fused_computation.7 | convolution fusion | flops 806682624 | bytes 5636096 | tf_op jit(solution)/shard_map/dot_general | solution.py:114
  222.4 6.4 %add_convert_fusion = bf16[384,2048]{1,0:T(8,128)(2,1)} fusion(bf16[384,2048]{1,0:T(8,128)(2,1)} %convolution_convert_fusion.1, bf16[384,2048]{1,0:T(8,128)(2,1)} %convolution_convert_fusion.2, bf16[384,2048]{1,0:T(8,128)(2,1)} %convolution_convert_fusion.3, bf16[4,256,2048]{2,1,0:T(8,128)(2,1)} %all-to-all-done.2, bf16[384,2048]{1,0:T(8,128)(2,1)} %reshape.209, ...), kind=kOutput, calls=%fused_computation.3 | convolution fusion | flops 812974080 | bytes 10354688 | tf_op jit(solution)/shard_map/dot_general | solution.py:114
  228.8 3.7 %reshape.210 = bf16[64,1,6,2048]{3,2,0,1:T(8,128)(2,1)} reshape(bf16[384,2048]{1,0:T(8,128)(2,1)} %add_convert_fusion) | data formatting | bytes 3145728 | tf_op jit(solution)/shard_map/reshape | solution.py:116
  232.5 7.2 %all-to-all-start.3 = ((bf16[64,1,6,2048]{3,2,1,0:T(8,128)(2,1)}), bf16[64,1,6,2048]{3,2,1,0:T(8,128)(2,1)}, u32[]{:S(2)}, u32[]{:S(2)}) async-start(bf16[64,1,6,2048]{3,2,1,0:T(8,128)(2,1)} %bitcast.84), calls=%async_computation.3 | async-start | bytes 4194304 | tf_op jit(solution)/shard_map/all_to_all | solution.py:117
  240.1 50.7 %all-to-all-done.3 = bf16[64,1,6,2048]{3,2,1,0:T(8,128)(2,1)} async-done(((bf16[64,1,6,2048]{3,2,1,0:T(8,128)(2,1)}), bf16[64,1,6,2048]{3,2,1,0:T(8,128)(2,1)}, u32[]{:S(2)}, u32[]{:S(2)}) %all-to-all-start.3) | async-done | bytes 1572896 | tf_op jit(solution)/shard_map/all_to_all | solution.py:117
  290.8 3.7 %reshape.211 = bf16[384,2048]{1,0:T(8,128)(2,1)} reshape(bf16[64,1,6,2048]{3,2,1,0:T(8,128)(2,1)} %all-to-all-done.3) | data formatting | bytes 3145728 | tf_op jit(solution)/shard_map/reshape | solution.py:118
  294.5 4.9 %gather_fusion.1 = bf16[256,2048]{1,0:T(8,128)(2,1)} fusion(bf16[384,2048]{1,0:T(8,128)(2,1)} %reshape.211, s32[1024]{0:T(1024)S(1)} %pad_clamp_fusion), kind=kCustom, calls=%fused_computation.1 | custom fusion | bytes 2098176 | tf_op jit(solution)/shard_map/gather | solution.py:119
  299.4 3.4 %reshape.212 = f32[128,2,2048]{2,1,0:T(2,128)} reshape(bf16[256,2048]{1,0:T(8,128)(2,1)} %gather_fusion.1) | data formatting | bytes 3145728 | tf_op jit(solution)/shard_map/convert_element_type | solution.py:119
  302.8 4.8 %multiply_reduce_fusion = f32[128,2048]{1,0:T(8,128)S(1)} fusion(f32[128,2,2048]{2,1,0:T(2,128)} %reshape.212, f32[128,2]{1,0:T(8,128)S(1)} %copy.26), kind=kLoop, calls=%fused_computation.9 | loop fusion | flops 786432 | bytes 3146752 | tf_op jit(solution)/shard_map/reduce_sum | solution.py:120
  (59 shorter events, 18.8 us)
Async XLA Ops:
  6.5 10.2 %copy-start = (bf16[512,2048]{1,0:T(8,128)(2,1)S(1)}, bf16[512,2048]{1,0:T(8,128)(2,1)}, u32[]{:S(2)}) copy-start(bf16[512,2048]{1,0:T(8,128)(2,1)} %param.17) | copy-start | bytes 6291460
  6.5 156.8 %all-gather.3.cloned.1.call-start = ((), (), s32[]{:S(2)}) async-start(), calls=%async_computation.4 | async-start | bytes 5242880 | tf_op jit(solution)/shard_map/all_gather | solution.py:63
  8.1 6.2 %collective-permute-start.1 = (bf16[15]{0:T(256)(128)(2,1)S(1)}, bf16[15]{0:T(256)(128)(2,1)S(1)}, u32[]{:S(2)}, u32[]{:S(2)}) collective-permute-start(bf16[15]{0:T(256)(128)(2,1)S(1)} %slice.144), channel_id=1, source_target_pairs={{0,4},{4,8},{8,12},{12,16},{16,20},{20,24},{24,28},{28,32},{32,36}... | collective-permute-start | bytes 98 | tf_op jit(solution)/shard_map/ppermute | solution.py:13
  10.7 5.0 %collective-permute-start = (bf16[15,256]{1,0:T(8,128)(2,1)S(1)}, bf16[15,256]{1,0:T(8,128)(2,1)S(1)}, u32[]{:S(2)}, u32[]{:S(2)}) collective-permute-start(bf16[15,256]{1,0:T(8,128)(2,1)S(1)} %slice.142), channel_id=1, source_target_pairs={{0,4},{4,8},{8,12},{12,16},{16,20},{20,24},{24,28},{28,32},{32,36}... | collective-permute-start | bytes 23048 | tf_op jit(solution)/shard_map/ppermute | solution.py:13
  22.0 54.4 %all-to-all-start = ((bf16[4,128,2048]{2,1,0:T(8,128)(2,1)}), bf16[4,128,2048]{2,1,0:T(8,128)(2,1)}, u32[]{:S(2)}, u32[]{:S(2)}) async-start(bf16[4,128,2048]{2,1,0:T(8,128)(2,1)} %bitcast.85), calls=%async_computation | async-start | bytes 4194304 | tf_op jit(solution)/shard_map/all_to_all | solution.py:23
  26.6 180.4 %all-gather.5.cloned.1.call-start = ((), (), s32[]{:S(2)}) async-start(), calls=%async_computation.5 | async-start | bytes 5242880 | tf_op jit(solution)/shard_map/all_gather | solution.py:64
  30.2 49.6 %copy-start.3 = (f32[2048]{0:T(1024)S(1)}, f32[2048]{0:T(1024)}, u32[]{:S(2)}) copy-start(f32[2048]{0:T(1024)} %param.18) | copy-start | bytes 24580
  88.7 63.2 %copy-start.2 = (bf16[1,256,2048]{2,1,0:T(8,128)(2,1)S(1)}, bf16[1,256,2048]{2,1,0:T(8,128)(2,1)}, u32[]{:S(2)}) copy-start(bf16[1,256,2048]{2,1,0:T(8,128)(2,1)} %param.23) | copy-start | bytes 3145732
  154.5 52.6 %all-to-all-start.2 = ((bf16[4,256,2048]{2,1,0:T(8,128)(2,1)}), bf16[4,256,2048]{2,1,0:T(8,128)(2,1)}, u32[]{:S(2)}, u32[]{:S(2)}) async-start(bf16[4,256,2048]{2,1,0:T(8,128)(2,1)} %concatenate.11), calls=%async_computation.2 | async-start | bytes 8388608 | tf_op jit(solution)/shard_map/all_to_all | solution.py:65
  163.3 3.1 copy-start.1
  166.4 2.7 copy-start.5
  232.5 7.4 %copy-start.4 = (f32[128,2]{0,1:T(2,128)S(1)}, f32[128,2]{0,1:T(2,128)}, u32[]{:S(2)}) copy-start(f32[128,2]{0,1:T(2,128)} %param.20) | copy-start | bytes 3076
  232.5 58.3 %all-to-all-start.3 = ((bf16[64,1,6,2048]{3,2,1,0:T(8,128)(2,1)}), bf16[64,1,6,2048]{3,2,1,0:T(8,128)(2,1)}, u32[]{:S(2)}, u32[]{:S(2)}) async-start(bf16[64,1,6,2048]{3,2,1,0:T(8,128)(2,1)} %bitcast.84), calls=%async_computation.3 | async-start | bytes 4194304 | tf_op jit(solution)/shard_map/all_to_all | solution.py:117
Sparse Core Ops, SparseCore 0:
  9.1 76.1 all-gather.2
  87.2 51.1 all-gather.4
